TPU v7x, 32 devices: a whole 2x2x4 slice. The times are simulated.
32 devices in a mesh: grp: 2 (over y), sp: 4 (over z), tp: 4 (over x, core).
Axes of the slice: x: 2, y: 2, z: 4, core: 2. Of those that a mesh axis runs over, the one named last changes fastest.
Arguments:
- residual: bfloat16 [2048, 2048], P(('grp', 'sp')), parts along dimension 0, may hold values from -6 to 6
- queries: bfloat16 [2048, 1024], P(('grp', 'sp'), 'tp'), parts along dimension 0, may hold values from -400 to 400
- keys: bfloat16 [2048, 1024], P(('grp', 'sp'), 'tp'), parts along dimension 0, may hold values from -8 to 8
- values: bfloat16 [2048, 1024], P(('grp', 'sp'), 'tp'), parts along dimension 0, may hold values from -6 to 6
- log_gates: float32 [2048, 16], P(('grp', 'sp'), 'tp'), parts along dimension 0, may hold values from -126 to 0, as said below
- w_out: bfloat16 [1024, 2048], P('tp'), may hold values from -0.75 to 0.75
- norm_gain: float32 [2048], replicated, may hold values from 0.1 to 1.9
- w_gate: bfloat16 [2048, 5632], P('sp', 'tp'), may hold values from -0.125 to 0.125
- w_up: bfloat16 [2048, 5632], P('sp', 'tp'), may hold values from -0.125 to 0.125
- w_down: bfloat16 [5632, 2048], P('tp', 'sp'), may hold values from -0.078125 to 0.078125
Outputs:
- output: bfloat16 [2048, 2048], P(('grp', 'sp', 'tp')), parts along dimension 0
There are 2 independent parts, one for each index of `grp`. A program takes and returns all parts, laid end to end along the dimension named above; an argument that names none is the same for every part. Nothing has to cross between parts.
Inputs may be any that keep to these rules, and one draw needn't show every extreme that they name: `log_gates`: never rises along positions.
All inputs are finite; a program needn't handle non-finite values.
Results may differ from a plain program's by a relative error of at most 0.014.
Values may be sent and summed in bfloat16 or wider, within the bound.
A program may use at most 128 MiB of HBM per device.

v0:
```python
import math

import jax
import jax.numpy as jnp
from jax import lax
from jax.sharding import PartitionSpec as P


def normalize(rows_in, gain):
    floats = rows_in.astype(jnp.float32)
    scaled = floats * lax.rsqrt(jnp.mean(floats * floats, axis=-1, keepdims=True) + 1e-06)
    return (scaled * gain).astype(jnp.bfloat16)


def attend(queries, keys, values, log_gates):
    row_count = queries.shape[0]
    head_count = log_gates.shape[1]
    head_width = queries.shape[1] // head_count
    score_scale = head_width ** (-0.5)
    first_row = lax.axis_index("sp") * row_count
    query_heads = queries.reshape(row_count, head_count, head_width)
    query_gates = log_gates.T
    query_positions = first_row + jnp.arange(row_count, dtype=jnp.int32)
    initial = (
        jnp.full((head_count, row_count), -1e30, jnp.float32),
        jnp.zeros((head_count, row_count), jnp.float32),
        jnp.zeros((head_count, row_count, head_width), jnp.float32),
    )
    carried = initial
    key_piece = lax.all_gather(keys.astype(jnp.float32), "sp", axis=0, tiled=True).astype(
        jnp.bfloat16
    )
    value_piece = lax.all_gather(values.astype(jnp.float32), "sp", axis=0, tiled=True).astype(
        jnp.bfloat16
    )
    gate_piece = lax.all_gather(log_gates, "sp", axis=0, tiled=True)
    length = key_piece.shape[0]
    block_rows = math.gcd(length, 2048)
    block_count = length // block_rows
    key_blocks = key_piece.reshape(block_count, block_rows, head_count, head_width)
    value_blocks = value_piece.reshape(block_count, block_rows, head_count, head_width)
    gate_blocks = gate_piece.reshape(block_count, block_rows, head_count)
    offsets = jnp.arange(block_count, dtype=jnp.int32) * block_rows

    def one_block(state, inputs):
        current_key_block, value_block, gate_block, offset = inputs

        def work(current):
            running_max, running_sum, accumulated = current
            scores = (
                jnp.einsum(
                    "qhd,khd->hqk",
                    query_heads,
                    current_key_block,
                    preferred_element_type=jnp.float32,
                )
                * score_scale
            )
            scores = scores + query_gates[:, :, None] - gate_block.T[:, None, :]
            key_positions = offset + jnp.arange(block_rows, dtype=jnp.int32)
            causal = (query_positions[:, None] >= key_positions[None, :])[None]
            scores = jnp.where(causal, scores, -1e30)
            new_max = jnp.maximum(running_max, jnp.max(scores, axis=-1))
            weights = jnp.where(causal, jnp.exp(scores - new_max[:, :, None]), 0.0)
            rescale = jnp.exp(running_max - new_max)
            running_sum = running_sum * rescale + jnp.sum(weights, axis=-1)
            product = jnp.einsum(
                "hqk,khd->hqd",
                weights.astype(jnp.bfloat16),
                value_block,
                preferred_element_type=jnp.float32,
            )
            accumulated = accumulated * rescale[:, :, None] + product
            return (new_max, running_sum, accumulated)

        state = lax.cond(offset <= first_row + row_count - 1, work, lambda current: current, state)
        return (state, None)

    carried, _ = lax.scan(one_block, carried, (key_blocks, value_blocks, gate_blocks, offsets))
    running_max, running_sum, accumulated = carried
    attended = accumulated / running_sum[:, :, None]
    return (
        attended.transpose(1, 0, 2).reshape(row_count, head_count * head_width).astype(jnp.bfloat16)
    )


def body(residual, queries, keys, values, log_gates, w_out, norm_gain, w_gate, w_up, w_down):
    attended = attend(queries, keys, values, log_gates)
    row_count = attended.shape[0]
    per_device = row_count // lax.axis_size("tp")
    my_first = lax.axis_index("tp") * per_device
    projected = lax.psum(
        jnp.dot(attended, w_out, preferred_element_type=jnp.float32).astype(jnp.bfloat16), "tp"
    ).astype(jnp.float32)
    mixed_all = (residual.astype(jnp.float32) + projected).astype(jnp.bfloat16)
    normed_all = normalize(mixed_all, norm_gain)
    mixed = lax.dynamic_slice_in_dim(mixed_all, my_first, per_device, 0)
    gate_whole = lax.all_gather(w_gate, "sp", axis=0, tiled=True)
    up_whole = lax.all_gather(w_up, "sp", axis=0, tiled=True)
    down_whole = lax.all_gather(w_down, "sp", axis=1, tiled=True)
    gate_proj = jnp.dot(normed_all, gate_whole, preferred_element_type=jnp.float32)
    up_proj = jnp.dot(normed_all, up_whole, preferred_element_type=jnp.float32)
    hidden = (jax.nn.silu(gate_proj) * up_proj).astype(jnp.bfloat16)
    down_sum = lax.psum_scatter(
        jnp.dot(hidden, down_whole, preferred_element_type=jnp.float32).astype(jnp.bfloat16),
        "tp",
        scatter_dimension=0,
        tiled=True,
    ).astype(jnp.float32)
    summed = mixed.astype(jnp.float32) + 0.5 * down_sum
    scaled = summed * lax.rsqrt(jnp.mean(summed * summed, axis=-1, keepdims=True) + 1e-06)
    return scaled.astype(jnp.bfloat16)


def solution(mesh):
    in_specs = (
        P(("grp", "sp"), None),
        P(("grp", "sp"), "tp"),
        P(("grp", "sp"), "tp"),
        P(("grp", "sp"), "tp"),
        P(("grp", "sp"), "tp"),
        P("tp", None),
        P(),
        P("sp", "tp"),
        P("sp", "tp"),
        P("tp", "sp"),
    )
    out_specs = P(("grp", "sp", "tp"), None)
    return jax.shard_map(body, mesh=mesh, in_specs=in_specs, out_specs=out_specs, check_vma=False)
```

profile of v0, /device:TPU:17, one launch (start us, length us, event | category | flops | bytes accessed | tf_op | source)
XLA Modules:
  0.0 427.9 jit_solution(2206887288210929115)
XLA Ops:
  7.4 1.1 copy.12
  8.5 12.8 %all_gather.18 = bf16[1024,256]{0,1:T(8,128)(2,1)S(1)} all-gather(bf16[256,256]{0,1:T(8,128)(2,1)S(1)} %copy.12), channel_id=1, replica_groups=mesh['grp'=2,'sp'=4,'tp'=4] {'sp'}, dimensions={0}, use_global_device_ids=true | all-gather | bytes 655360 | tf_op jit(solution)/shard_map/all_gather | solution.py:30
  21.3 1.0 copy.13
  22.3 11.7 %all_gather.20 = bf16[1024,256]{0,1:T(8,128)(2,1)S(1)} all-gather(bf16[256,256]{0,1:T(8,128)(2,1)S(1)} %copy.13), channel_id=1, replica_groups=mesh['grp'=2,'sp'=4,'tp'=4] {'sp'}, dimensions={0}, use_global_device_ids=true | all-gather | bytes 655360 | tf_op jit(solution)/shard_map/all_gather | solution.py:33
  34.0 10.9 %all_gather.19 = f32[1024,4]{0,1:T(4,128)S(1)} all-gather(f32[256,4]{0,1:T(4,128)} %param.16), channel_id=1, replica_groups=mesh['grp'=2,'sp'=4,'tp'=4] {'sp'}, dimensions={0}, use_global_device_ids=true | all-gather | bytes 20480 | tf_op jit(solution)/shard_map/all_gather | solution.py:36
  45.0 7.0 %conditional.1 = ((f32[4,256]{1,0:T(4,128)S(1)}, f32[4,256,64]{1,2,0:T(8,128)S(1)})) conditional(s32[]{:T(128)} %convert_element_type.64, (f32[4,256]{1,0:T(4,128)S(1)}, f32[4,256,64]{1,2,0:T(8,128)S(1)}) %tuple.22, (s32[]{:T(128)}, s32[256]{0:T(256)S(1)}, bf16[256,256]{1,0:T(8,128)(2,1)}, bf16[1024,256]{0,1:T(8,128)(2,1)S(1)}, f32[4,256]{1,0:T(4,128)}, ...), branch_computations={%region_0.1_spmd, %region_1.0_spmd} | conditional | flops 288754944 | bytes 15727672 | solution.py:76
  45.0 0.0 copy-start.2
  45.0 0.2 iota_compare_fusion
  45.2 1.0 copy.14
  46.2 2.1 fusion.2
  48.3 2.0 fusion.1
  50.3 1.6 fusion.6
  52.0 1.4 convolution_convert_fusion
  53.5 0.0 all-reduce.2.cloned.1.call-update
  53.5 0.0 all-gather.4.cloned.1.call-start
  53.5 0.5 all-gather.4.cloned.1.call-update
  54.1 0.0 all-gather.6.cloned.1.call-start
  54.1 0.5 all-gather.6.cloned.1.call-update
  54.6 0.0 all-gather.8.cloned.1.call-start
  54.7 0.5 all-gather.8.cloned.1.call-update
  55.2 0.0 reduce-scatter.2.cloned.1.call-start
  55.3 44.5 %all-reduce.2.cloned.1.call-done = bf16[256,2048]{1,0:T(8,128)(2,1)} async-done(((bf16[256,2048]{1,0:T(8,128)(2,1)}), bf16[256,2048]{1,0:T(8,128)(2,1)}) %all-reduce.2.cloned.1.call-update) | async-done | bytes 1048592 | tf_op jit(solution)/shard_map/psum | solution.py:92
  99.8 1.7 fusion.13
  101.6 69.0 %all-gather.4.cloned.1.call-done = bf16[2048,1408]{1,0:T(8,128)(2,1)} async-done(((bf16[512,1408]{1,0:T(8,128)(2,1)}), bf16[2048,1408]{1,0:T(8,128)(2,1)}) %all-gather.4.cloned.1.call-update) | async-done | bytes 5767184 | tf_op jit(solution)/shard_map/all_gather | solution.py:98
  170.5 5.6 %fusion.18 = f32[256,1408]{1,0:T(8,128)} fusion(bf16[2048,1408]{1,0:T(8,128)(2,1)} %all-gather.4.cloned.1.call-done, bf16[256,2048]{1,0:T(8,128)(2,1)S(1)} %get-tuple-element.132, f32[2048]{0:T(1024)S(1)} %copy-done.3, f32[256]{0:T(256)S(1)} %add_rsqrt_fusion), kind=kOutput, calls=%fused_computation.29 | convolution fusion | flops 1478492160 | bytes 8266752 | tf_op jit(solution)/shard_map/dot_general | solution.py:101
  176.2 100.6 %all-gather.6.cloned.1.call-done = bf16[2048,1408]{1,0:T(8,128)(2,1)} async-done(((bf16[512,1408]{1,0:T(8,128)(2,1)}), bf16[2048,1408]{1,0:T(8,128)(2,1)}) %all-gather.6.cloned.1.call-update) | async-done | bytes 5767184 | tf_op jit(solution)/shard_map/all_gather | solution.py:99
  276.8 106.3 %all-gather.8.cloned.1.call-done = bf16[1408,2048]{1,0:T(8,128)(2,1)} async-done(((bf16[1408,512]{1,0:T(8,128)(2,1)}), bf16[1408,2048]{1,0:T(8,128)(2,1)}) %all-gather.8.cloned.1.call-update) | async-done | bytes 5767184 | tf_op jit(solution)/shard_map/all_gather | solution.py:100
  383.1 9.3 %convolution_convert_fusion.1 = bf16[256,2048]{1,0:T(8,128)(2,1)} fusion(bf16[1408,2048]{1,0:T(8,128)(2,1)} %all-gather.8.cloned.1.call-done, bf16[2048,1408]{1,0:T(8,128)(2,1)} %all-gather.6.cloned.1.call-done, f32[256,1408]{1,0:T(8,128)} %fusion.18, bf16[256,2048]{1,0:T(8,128)(2,1)S(1)} %get-tuple-element.132, f32[2048]{0:T(1024)S(1)} %copy-done.3, ...), kind=kOutput, calls=%fused_computation.21 | convolution fusion | flops 2957574144 | bytes 15082496 | tf_op jit(solution)/shard_map/dot_general | solution.py:105
  392.3 0.0 reduce-scatter.2.cloned.1.call-update
  392.4 25.0 %reduce-scatter.2.cloned.1.call-done = bf16[64,2048]{1,0:T(8,128)(2,1)} async-done(((bf16[256,2048]{1,0:T(8,128)(2,1)}), bf16[64,2048]{1,0:T(8,128)(2,1)}) %reduce-scatter.2.cloned.1.call-update) | async-done | bytes 262160 | tf_op jit(solution)/shard_map/reduce_scatter | solution.py:104
  417.4 1.2 multiply_reduce_fusion
  418.6 1.8 multiply_convert_fusion
  (17 shorter events, 0.1 us)
Async XLA Ops:
  7.4 44.6 %copy-start = (bf16[256,2048]{1,0:T(8,128)(2,1)S(1)}, bf16[256,2048]{1,0:T(8,128)(2,1)}, u32[]{:S(2)}) copy-start(bf16[256,2048]{1,0:T(8,128)(2,1)} %param.17) | copy-start | bytes 3145732
  7.4 92.4 %all-reduce.2.cloned.1.call-start = ((), (), s32[]{:S(2)}) async-start(), calls=%async_computation.1 | async-start | bytes 2097152 | tf_op jit(solution)/shard_map/psum | solution.py:92
  45.0 3.3 copy-start.2
  52.0 47.9 %copy-start.1 = (bf16[256,2048]{1,0:T(8,128)(2,1)S(1)}, bf16[256,2048]{1,0:T(8,128)(2,1)}, u32[]{:S(2)}) copy-start(bf16[256,2048]{1,0:T(8,128)(2,1)} %param.12) | copy-start | bytes 3145732
  53.4 117.1 %copy-start.3 = (f32[2048]{0:T(1024)S(1)}, f32[2048]{0:T(1024)}, u32[]{:S(2)}) copy-start(f32[2048]{0:T(1024)} %param.18) | copy-start | bytes 24580
  53.5 117.1 %all-gather.4.cloned.1.call-start = ((), (), s32[]{:S(2)}) async-start(), calls=%async_computation.2 | async-start | bytes 7208960 | tf_op jit(solution)/shard_map/all_gather | solution.py:98
  54.1 222.7 %all-gather.6.cloned.1.call-start = ((), (), s32[]{:S(2)}) async-start(), calls=%async_computation.3 | async-start | bytes 7208960 | tf_op jit(solution)/shard_map/all_gather | solution.py:99
  54.6 328.4 %all-gather.8.cloned.1.call-start = ((), (), s32[]{:S(2)}) async-start(), calls=%async_computation.4 | async-start | bytes 7208960 | tf_op jit(solution)/shard_map/all_gather | solution.py:100
  55.2 362.2 %reduce-scatter.2.cloned.1.call-start = ((), (), s32[]{:S(2)}) async-start(), calls=%async_computation.5 | async-start | bytes 1310720 | tf_op jit(solution)/shard_map/reduce_scatter | solution.py:104
Sparse Core Ops, SparseCore 0:
  53.6 46.1 all-reduce.1
  392.5 24.8 reduce-scatter.1
Sparse Core Ops, SparseCore 1:
  55.5 114.9 all-gather.3
  172.0 104.8 all-gather.5
  278.2 104.8 all-gather.7
where the time goes:
time: 430 us; the launch traced here: 428 us
  waiting for transfers between devices  347 us (81%)
  blocking collectives  35.4 us (8%)
  matrix products  20 us (5%)
  between operations  15.1 us (4%)
  other arithmetic  6.94 us (2%)
    all_gather x1, waiting for transfers between devices, body(): down_whole = lax.all_gather(w_down, 'sp', axis=1, tiled=True)  106 us
    all_gather x1, waiting for transfers between devices, body(): up_whole = lax.all_gather(w_up, 'sp', axis=0, tiled=True)  101 us
    all_gather x1, waiting for transfers between devices, body(): gate_whole = lax.all_gather(w_gate, 'sp', axis=0, tiled=True)  69 us
    psum x1, waiting for transfers between devices, body(): lax.psum(jnp.dot(attended, w_out, preferred_element_type=jnp.float32).ast...  44.5 us
    reduce_scatter x1, waiting for transfers between devices, body(): lax.psum_scatter(jnp.dot(hidden, down_whole, preferred_element_type=jnp.f...  25 us
    all_gather x1, blocking collectives, attend(): lax.all_gather(keys.astype(jnp.float32), 'sp', axis=0, tiled=True)  12.8 us
    all_gather x1, blocking collectives, attend(): lax.all_gather(values.astype(jnp.float32), 'sp', axis=0, tiled=True)  11.7 us
    all_gather x1, blocking collectives, attend(): gate_piece = lax.all_gather(log_gates, 'sp', axis=0, tiled=True)  10.9 us
  transfers between devices with their start and end apart: 5, of which 5 were waited for; matrix products, arithmetic and copies ran while one was open for 2% of the time, Pallas kernels for 0%

commit v1 on v0

--- a/solution.py
+++ b/solution.py
@@ -1,8 +1,11 @@
+import functools
 import math
 
 import jax
 import jax.numpy as jnp
 from jax import lax
+from jax.experimental import pallas as pl
+from jax.experimental.pallas import tpu as pltpu
 from jax.sharding import PartitionSpec as P
 
 
@@ -112,6 +115,417 @@
     return scaled.astype(jnp.bfloat16)
 
 
+MESH = pl.DeviceIdType.MESH
+
+
+def send(src, dst, sems, index, target):
+    return pltpu.make_async_remote_copy(
+        src_ref=src,
+        dst_ref=dst,
+        send_sem=sems.at[(0, *index)],
+        recv_sem=sems.at[(1, *index)],
+        device_id=target,
+        device_id_type=MESH,
+    )
+
+
+def layer_kernel(
+    n, tp, chunk,
+    q_ref, k_ref, v_ref, g_ref, gt_ref, residual_ref, w_out_ref, gain_ref, wg_ref, wu_ref, wd_ref,
+    out_ref,
+    k_all, v_all, gt_all, att, proj, pc_buf, px_send, px_buf, mixed, normed,
+    wg_all, wu_all, wd_all, hid, part, c_buf, x_send, x_buf, z_send, z_buf,
+    kv_sems, w_sems, y_sems, pc_sems, px_sems, nz_sems, nx_sems, nc_sems, c_sems, x_sems, z_sems,
+):
+    me = lax.axis_index("sp")
+    t = lax.axis_index("tp")
+    g = lax.axis_index("grp")
+    x, c = t // 2, t % 2
+    nx = tp // 2
+    mate = x * 2 + (1 - c)
+    rows = q_ref.shape[0]
+    sub = rows // tp
+    width = residual_ref.shape[1]
+    heads = g_ref.shape[1]
+    head = q_ref.shape[1] // heads
+    depth = wg_ref.shape[0]
+    ff = wg_ref.shape[1]
+    half = depth // 2
+    dcols = wd_ref.shape[1]
+    dhalf = dcols // 2
+
+    def there(d):
+        return lax.rem(me + d, n)
+
+    def origin(d):
+        return lax.rem(me + n - d, n)
+
+    def across(dx):
+        return lax.rem(x + dx, nx)
+
+    barrier = pltpu.get_barrier_semaphore()
+    for d in range(1, n):
+        pl.semaphore_signal(barrier, inc=1, device_id={"sp": there(d)}, device_id_type=MESH)
+    for dx in range(1, nx):
+        pl.semaphore_signal(
+            barrier, inc=1, device_id={"tp": across(dx) * 2 + c}, device_id_type=MESH
+        )
+    pl.semaphore_signal(barrier, inc=1, device_id={"tp": mate}, device_id_type=MESH)
+    pl.semaphore_signal(barrier, inc=1, device_id={"grp": 1 - g}, device_id_type=MESH)
+    pl.semaphore_wait(barrier, n - 1 + nx - 1 + 2)
+
+    def kv_copies(d):
+        target = {"sp": there(d)}
+        return (
+            send(k_ref, k_all.at[d - 1], kv_sems, (d - 1, 0), target),
+            send(v_ref, v_all.at[d - 1], kv_sems, (d - 1, 1), target),
+            send(gt_ref, gt_all.at[d - 1], kv_sems, (d - 1, 2), target),
+        )
+
+    for d in range(1, n):
+
+        @pl.when(me + d < n)
+        def _(d=d):
+            for copy in kv_copies(d):
+                copy.start()
+
+    def w_copies(d):
+        j = there(d)
+        start = pl.multiple_of(jnp.minimum(j * chunk, ff - chunk), 128)
+        target = {"sp": j}
+        in_rows = pl.ds(pl.multiple_of(g * half, half), half)
+        in_cols = pl.ds(pl.multiple_of(g * dhalf, dhalf), dhalf)
+        return (
+            send(wg_ref.at[in_rows, pl.ds(start, chunk)], wg_all.at[d, in_rows], w_sems, (d - 1, 0), target),
+            send(wu_ref.at[in_rows, pl.ds(start, chunk)], wu_all.at[d, in_rows], w_sems, (d - 1, 1), target),
+            send(wd_ref.at[pl.ds(start, chunk), in_cols], wd_all.at[d, :, in_cols], w_sems, (d - 1, 2), target),
+        )
+
+    def y_copies(d):
+        target = {"grp": 1 - g}
+        in_rows = pl.ds(pl.multiple_of(g * half, half), half)
+        in_cols = pl.ds(pl.multiple_of(g * dhalf, dhalf), dhalf)
+        return (
+            send(wg_all.at[d, in_rows], wg_all.at[d, in_rows], y_sems, (d - 1, 0), target),
+            send(wu_all.at[d, in_rows], wu_all.at[d, in_rows], y_sems, (d - 1, 1), target),
+            send(wd_all.at[d, :, in_cols], wd_all.at[d, :, in_cols], y_sems, (d - 1, 2), target),
+        )
+
+    for d in range(1, n):
+        for copy in w_copies(d):
+            copy.start()
+
+    mine = pl.multiple_of(jnp.minimum(me * chunk, ff - chunk), 128)
+    wg_all[0] = wg_ref[:, pl.ds(mine, chunk)]
+    wu_all[0] = wu_ref[:, pl.ds(mine, chunk)]
+    wd_all[0] = wd_ref[pl.ds(mine, chunk), :]
+
+    for d in range(1, n):
+
+        @pl.when(me + d < n)
+        def _(d=d):
+            for copy in kv_copies(d):
+                copy.wait_send()
+
+        @pl.when(me >= d)
+        def _(d=d):
+            for copy in kv_copies(d):
+                copy.wait_recv()
+
+        @pl.when(me < d)
+        def _(d=d):
+            k_all[d - 1] = jnp.zeros_like(k_ref)
+            v_all[d - 1] = jnp.zeros_like(v_ref)
+            gt_all[d - 1] = jnp.zeros_like(gt_ref)
+
+    pair = 128 // head
+    lane = lax.broadcasted_iota(jnp.int32, (rows, 128), 1)
+    causal = lax.broadcasted_iota(jnp.int32, (rows, rows), 0) >= lax.broadcasted_iota(
+        jnp.int32, (rows, rows), 1
+    )
+    contract = (((1,), (1,)), ((), ()))
+    for p in range(heads // pair):
+        cols = slice(p * 128, (p + 1) * 128)
+        q_pair = q_ref[:, cols]
+        joined = jnp.zeros((rows, 128), jnp.float32)
+        for i in range(pair):
+            h = p * pair + i
+            inside = (lane >= i * head) & (lane < (i + 1) * head)
+            q_head = jnp.where(inside, q_pair, jnp.zeros_like(q_pair))
+            g_query = g_ref[:, h : h + 1]
+            scores = []
+            for d in range(n):
+                k_pair = k_ref[:, cols] if d == 0 else k_all[d - 1, :, cols]
+                g_key = gt_ref[h : h + 1, :] if d == 0 else gt_all[d - 1, h : h + 1, :]
+                score = (
+                    lax.dot_general(q_head, k_pair, contract, preferred_element_type=jnp.float32)
+                    * head ** (-0.5)
+                    + g_query
+                    - g_key
+                )
+                allowed = causal if d == 0 else (jnp.zeros((rows, rows), jnp.int32) + me) >= d
+                scores.append(jnp.where(allowed, score, -1e30))
+            peak = functools.reduce(
+                jnp.maximum, [jnp.max(score, axis=-1, keepdims=True) for score in scores]
+            )
+            total = jnp.zeros((rows, 1), jnp.float32)
+            summed = jnp.zeros((rows, 128), jnp.float32)
+            for d in range(n):
+                v_pair = v_ref[:, cols] if d == 0 else v_all[d - 1, :, cols]
+                weight = jnp.exp(scores[d] - peak)
+                total += jnp.sum(weight, axis=-1, keepdims=True)
+                summed += jnp.dot(
+                    weight.astype(jnp.bfloat16), v_pair, preferred_element_type=jnp.float32
+                )
+            joined = jnp.where(inside, summed / total, joined)
+        att[:, cols] = joined.astype(jnp.bfloat16)
+
+    for k in range(width // 512):
+        cols = slice(k * 512, (k + 1) * 512)
+        proj[:, cols] = jnp.dot(
+            att[...], w_out_ref[:, cols], preferred_element_type=jnp.float32
+        ).astype(jnp.bfloat16)
+
+    def block(index):
+        return pl.ds(pl.multiple_of(index * sub, sub), sub)
+
+    pc = [
+        send(proj.at[block(across(dx) * 2 + 1 - c)], pc_buf.at[dx], pc_sems, (dx,), {"tp": mate})
+        for dx in range(nx)
+    ]
+    for copy in pc:
+        copy.start()
+    px = [
+        send(px_send.at[dx], px_buf.at[dx], px_sems, (dx,), {"tp": across(dx) * 2 + c})
+        for dx in range(nx)
+    ]
+    for dx in range(1, nx):
+        pc[dx].wait_recv()
+        px_send[dx] = (
+            proj[block(across(dx) * 2 + c), :].astype(jnp.float32) + pc_buf[dx].astype(jnp.float32)
+        ).astype(jnp.bfloat16)
+        px[dx].start()
+    pc[0].wait_recv()
+    acc = proj[block(t), :].astype(jnp.float32) + pc_buf[0].astype(jnp.float32)
+    for dx in range(1, nx):
+        px[dx].wait_recv()
+        acc += px_buf[dx].astype(jnp.float32)
+    mix = (residual_ref[block(t), :].astype(jnp.float32) + acc).astype(jnp.bfloat16)
+    mixed[...] = mix
+    floats = mix.astype(jnp.float32)
+    scale = lax.rsqrt(jnp.mean(floats * floats, axis=-1, keepdims=True) + 1e-06)
+    normed[me, block(t), :] = (floats * scale * gain_ref[...]).astype(jnp.bfloat16)
+
+    own = normed.at[me, block(t)]
+    nz = [send(own, own, nz_sems, (d,), {"sp": there(d)}) for d in range(n)]
+    for d in range(1, n):
+        nz[d].start()
+
+    def spread(d):
+        piece = normed.at[origin(d), block(t)]
+        copies = [send(piece, piece, nc_sems, (d, 0), {"tp": mate})]
+        for dx in range(1, nx):
+            copies.append(send(piece, piece, nx_sems, (d, dx), {"tp": across(dx) * 2 + c}))
+        return copies
+
+    def relay(d, dx):
+        piece = normed.at[origin(d), block(lax.rem(x + nx - dx, nx) * 2 + c)]
+        return send(piece, piece, nc_sems, (d, dx), {"tp": mate})
+
+    spreads = [spread(d) for d in range(n)]
+    for copy in spreads[0]:
+        copy.start()
+    for d in range(1, n):
+        for copy, forward in zip(w_copies(d), y_copies(d)):
+            copy.wait_recv()
+            forward.start()
+    for dx in range(1, nx):
+        spreads[0][dx].wait_recv()
+        relay(0, dx).start()
+    for d in range(1, n):
+        nz[d].wait_recv()
+        for copy in spreads[d]:
+            copy.start()
+    for d in range(1, n):
+        for dx in range(1, nx):
+            spreads[d][dx].wait_recv()
+            relay(d, dx).start()
+    for d in range(1, n):
+        for copy in y_copies(d):
+            copy.wait_recv()
+    for d in range(n):
+        spreads[d][0].wait_recv()
+        for dx in range(1, nx):
+            relay(d, dx).wait_recv()
+
+    skipped = me * chunk - mine
+    live = lax.broadcasted_iota(jnp.int32, (rows, chunk), 1) >= skipped
+    order = [d % n for d in range(1, n + 1)]
+
+    def c_copy(d, dx):
+        j = there(d)
+        return send(
+            part.at[j, block(across(dx) * 2 + 1 - c)], c_buf.at[d, dx], c_sems, (d, dx), {"tp": mate}
+        )
+
+    def feed(index, carry):
+        d = lax.rem(index + 1, n)
+        j = there(d)
+        gate = jnp.zeros((rows, chunk), jnp.float32)
+        up = jnp.zeros((rows, chunk), jnp.float32)
+        for e in range(n):
+            piece = normed[j, :, pl.ds(pl.multiple_of(origin(e) * depth, depth), depth)]
+            gate += jnp.dot(piece, wg_all[e], preferred_element_type=jnp.float32)
+            up += jnp.dot(piece, wu_all[e], preferred_element_type=jnp.float32)
+        value = gate / (1.0 + jnp.exp(-gate)) * up
+        hid[...] = jnp.where(live, value, 0.0).astype(jnp.bfloat16)
+        for e in range(n):
+            part[j, :, pl.ds(pl.multiple_of(origin(e) * dcols, dcols), dcols)] = jnp.dot(
+                hid[...], wd_all[e], preferred_element_type=jnp.float32
+            ).astype(jnp.bfloat16)
+        for dx in range(nx):
+            c_copy(d, dx).start()
+        return carry
+
+    lax.fori_loop(0, n, feed, 0)
+
+    def x_copy(d, dx):
+        return send(x_send.at[d, dx], x_buf.at[d, dx], x_sems, (d, dx), {"tp": across(dx) * 2 + c})
+
+    def z_copy(d):
+        return send(z_send.at[d], z_buf.at[d], z_sems, (d,), {"sp": there(d)})
+
+    for d in order:
+        for dx in range(1, nx):
+            c_copy(d, dx).wait_recv()
+            x_send[d, dx] = (
+                part[there(d), block(across(dx) * 2 + c), :].astype(jnp.float32)
+                + c_buf[d, dx].astype(jnp.float32)
+            ).astype(jnp.bfloat16)
+            x_copy(d, dx).start()
+    for d in order:
+        c_copy(d, 0).wait_recv()
+        acc = part[there(d), block(t), :].astype(jnp.float32) + c_buf[d, 0].astype(jnp.float32)
+        for dx in range(1, nx):
+            x_copy(d, dx).wait_recv()
+            acc += x_buf[d, dx].astype(jnp.float32)
+        if d != 0:
+            z_send[d] = acc.astype(jnp.bfloat16)
+            z_copy(d).start()
+    for d in range(1, n):
+        z_copy(d).wait_recv()
+        acc += z_buf[d].astype(jnp.float32)
+    summed = mixed[...].astype(jnp.float32) + 0.5 * acc
+    scale = lax.rsqrt(jnp.mean(summed * summed, axis=-1, keepdims=True) + 1e-06)
+    out_ref[...] = (summed * scale).astype(jnp.bfloat16)
+
+    for copy in pc:
+        copy.wait_send()
+    for dx in range(1, nx):
+        px[dx].wait_send()
+    for d in range(n):
+        for copy in spreads[d]:
+            copy.wait_send()
+        for dx in range(1, nx):
+            relay(d, dx).wait_send()
+            x_copy(d, dx).wait_send()
+        for dx in range(nx):
+            c_copy(d, dx).wait_send()
+    for d in range(1, n):
+        nz[d].wait_send()
+        z_copy(d).wait_send()
+        for copy in w_copies(d):
+            copy.wait_send()
+        for copy in y_copies(d):
+            copy.wait_send()
+
+
+def fused_body(residual, queries, keys, values, log_gates, w_out, norm_gain, w_gate, w_up, w_down):
+    n, tp = lax.axis_size("sp"), lax.axis_size("tp")
+    rows, width = residual.shape
+    sub = rows // tp
+    nx = tp // 2
+    heads = log_gates.shape[1]
+    depth, ff = w_gate.shape
+    dcols = w_down.shape[1]
+    chunk = window(ff, n)
+    gates_t = jnp.pad(log_gates.T, ((0, -heads % 8), (0, 0)))
+    bf16, f32 = jnp.bfloat16, jnp.float32
+    shapes = [
+        ((n - 1, *keys.shape), bf16),
+        ((n - 1, *values.shape), bf16),
+        ((n - 1, *gates_t.shape), f32),
+        (queries.shape, bf16),
+        ((rows, width), bf16),
+        ((nx, sub, width), bf16),
+        ((nx, sub, width), bf16),
+        ((nx, sub, width), bf16),
+        ((sub, width), bf16),
+        ((n, rows, width), bf16),
+        ((n, depth, chunk), bf16),
+        ((n, depth, chunk), bf16),
+        ((n, chunk, dcols), bf16),
+        ((rows, chunk), bf16),
+        ((n, rows, width), bf16),
+        ((n, nx, sub, width), bf16),
+        ((n, nx, sub, width), bf16),
+        ((n, nx, sub, width), bf16),
+        ((n, sub, width), bf16),
+        ((n, sub, width), bf16),
+    ]
+    sems = [
+        (2, n - 1, 3),
+        (2, n - 1, 3),
+        (2, n - 1, 3),
+        (2, nx),
+        (2, nx),
+        (2, n),
+        (2, n, nx),
+        (2, n, nx),
+        (2, n, nx),
+        (2, n, nx),
+        (2, n),
+    ]
+    return pl.pallas_call(
+        functools.partial(layer_kernel, n, tp, chunk),
+        out_shape=jax.ShapeDtypeStruct((sub, width), bf16),
+        in_specs=[pl.BlockSpec(memory_space=pltpu.VMEM)] * 11,
+        out_specs=pl.BlockSpec(memory_space=pltpu.VMEM),
+        scratch_shapes=[pltpu.VMEM(shape, dtype) for shape, dtype in shapes]
+        + [pltpu.SemaphoreType.DMA(shape) for shape in sems],
+        compiler_params=pltpu.CompilerParams(
+            collective_id=0, has_side_effects=True, vmem_limit_bytes=60 * 1024 * 1024
+        ),
+    )(
+        queries, keys, values, log_gates, gates_t, residual, w_out, norm_gain[None, :],
+        w_gate, w_up, w_down,
+    )
+
+
+def window(ff, n):
+    return -(-ff // (n * 128)) * 128
+
+
+def fits(mesh, shapes):
+    residual, queries, gates, gate = shapes
+    n, tp, grp = mesh.shape["sp"], mesh.shape["tp"], mesh.shape["grp"]
+    ff = gate[1] // tp
+    heads = gates[1] // tp
+    head = queries[1] // gates[1]
+    rows = residual[0] // (grp * n)
+    return (
+        grp == 2
+        and 2 <= n <= 4
+        and tp % 2 == 0
+        and ff % 128 == 0
+        and window(ff, n) * (n - 1) < ff
+        and 128 % head == 0
+        and (heads * head) % 128 == 0
+        and rows % (16 * tp) == 0
+        and rows * n * residual[1] <= 1 << 21
+    )
+
+
 def solution(mesh):
     in_specs = (
         P(("grp", "sp"), None),
@@ -126,4 +540,13 @@
         P("tp", "sp"),
     )
     out_specs = P(("grp", "sp", "tp"), None)
-    return jax.shard_map(body, mesh=mesh, in_specs=in_specs, out_specs=out_specs, check_vma=False)
+
+    def layer(*args):
+        residual, queries, _, _, log_gates, _, _, w_gate, _, _ = args
+        shapes = (residual.shape, queries.shape, log_gates.shape, w_gate.shape)
+        chosen = fused_body if fits(mesh, shapes) else body
+        return jax.shard_map(
+            chosen, mesh=mesh, in_specs=in_specs, out_specs=out_specs, check_vma=False
+        )(*args)
+
+    return layer

time: 430 us -> 164 us (0.38)
  waiting for transfers between devices: 347 us -> 0 us
  Pallas kernels: 0 us -> 157 us
  blocking collectives: 35.4 us -> 0 us
  matrix products: 20 us -> 0 us
  between operations: 15.1 us -> 0.01 us
  other arithmetic: 6.94 us -> 0 us
    all_gather x3 -> x0, waiting for transfers between devices: 276 us -> none  [the longest x1 106 us: body(): down_whole = lax.all_gather(w_down, 'sp', axis=1, tiled=True)]
    pallas_call x0 -> x1, Pallas kernels: none -> 157 us  [fused_body(): pl.pallas_call(functools.partial(layer_kernel, n, tp, chunk), out_shape=j...]
    psum x1 -> x0, waiting for transfers between devices: 44.5 us -> none  [body(): lax.psum(jnp.dot(attended, w_out, preferred_element_type=jnp.float32).ast...]
    all_gather x3 -> x0, blocking collectives: 35.4 us -> none  [the longest x1 12.8 us: attend(): lax.all_gather(keys.astype(jnp.float32), 'sp', axis=0, tiled=True)]
    reduce_scatter x1 -> x0, waiting for transfers between devices: 25 us -> none  [body(): lax.psum_scatter(jnp.dot(hidden, down_whole, preferred_element_type=jnp.f...]
    dot_general x5 -> x0, matrix products: 20 us -> none  [the longest x1 9.26 us: body(): jnp.dot(hidden, down_whole, preferred_element_type=jnp.float32)]
    reduce_sum x3 -> x0, other arithmetic: 4.89 us -> none  [the longest x1 2.01 us: work(): running_sum = running_sum * rescale + jnp.sum(weights, axis=-1)]
  transfers between devices with their start and end apart: 5 -> 0, of which waited for: 5 -> 0; matrix products, arithmetic and copies ran while one was open for 2% -> 0% of each run, Pallas kernels for 0% -> 0%
where the time goes in v1:
time: 164 us; the launch traced here: 161 us
  Pallas kernels  157 us (96%)
  local copies, waits for them, and re-layouts  4.43 us (3%)
    pallas_call x1, Pallas kernels, fused_body(): pl.pallas_call(functools.partial(layer_kernel, n, tp, chunk), out_shape=j...  157 us

profile of v1, /device:TPU:17, one launch (start us, length us, event | category | flops | bytes accessed | tf_op | source)
XLA Modules:
  0.0 161.2 jit_solution(287909338874874142)
XLA Ops:
  0.0 1.3 pad.4.gt_ref
  1.3 1.5 copy.11.g_ref
  2.8 156.8 %shard_map.100 = bf16[64,2048]{1,0:T(8,128)(2,1)} custom-call(bf16[256,256]{1,0:T(8,128)(2,1)} %q_ref.1, bf16[256,256]{1,0:T(8,128)(2,1)} %k_ref.1, bf16[256,256]{1,0:T(8,128)(2,1)} %v_ref.1, f32[256,4]{1,0:T(8,128)} %copy.11.g_ref, f32[8,256]{1,0:T(8,128)} %pad.4.gt_ref, bf16[256,2048]{1,0:T(8,128)(2,1)} %residual_ref.1, bf16[256,2048]{1,0:T(8,128)(2,1)} %w_out_ref.1, ...), custom_call_target="tpu_custom_call" | custom-call | tf_op jit(solution)/shard_map/pallas_call | solution.py:489
  159.6 1.7 %copy.13 = bf16[64,2048]{1,0:T(8,128)(2,1)} copy(bf16[64,2048]{1,0:T(8,128)(2,1)} %shard_map.100) | data formatting | bytes 524288

commit v2 on v1

--- a/solution.py
+++ b/solution.py
@@ -175,62 +175,100 @@
     pl.semaphore_wait(barrier, n - 1 + nx - 1 + 2)
 
     def kv_copies(d):
-        target = {"sp": there(d)}
+        target = {"sp": lax.rem(me + 1, n)}
+        own = (k_ref, v_ref, gt_ref)
+        held = (k_all, v_all, gt_all)
+        return [
+            send(
+                own[i] if d == 1 else held[i].at[d - 2], held[i].at[d - 1], kv_sems, (d - 1, i), target
+            )
+            for i in range(3)
+        ]
+
+    @pl.when(me + 1 < n)
+    def _():
+        for copy in kv_copies(1):
+            copy.start()
+
+    last = ff - (n - 1) * chunk
+    my_rows = pl.ds(pl.multiple_of(g * half, half), half)
+    my_cols = pl.ds(pl.multiple_of(g * dhalf, dhalf), dhalf)
+
+    def w_copies(d, size):
+        j = there(d)
+        place = pl.ds(pl.multiple_of(jnp.minimum(j * chunk, ff - size), 128), size)
+        target = {"sp": j}
         return (
-            send(k_ref, k_all.at[d - 1], kv_sems, (d - 1, 0), target),
-            send(v_ref, v_all.at[d - 1], kv_sems, (d - 1, 1), target),
-            send(gt_ref, gt_all.at[d - 1], kv_sems, (d - 1, 2), target),
+            send(wg_ref.at[my_rows, place], wg_all.at[d, my_rows, :size], w_sems, (d - 1, 0), target),
+            send(wu_ref.at[my_rows, place], wu_all.at[d, my_rows, :size], w_sems, (d - 1, 1), target),
+            send(wd_ref.at[place, my_cols], wd_all.at[d, :size, my_cols], w_sems, (d - 1, 2), target),
         )
 
+    def y_copies(d, size):
+        target = {"grp": 1 - g}
+        gate = wg_all.at[d, my_rows, :size]
+        up = wu_all.at[d, my_rows, :size]
+        down = wd_all.at[d, :size, my_cols]
+        return (
+            send(gate, gate, y_sems, (d - 1, 0), target),
+            send(up, up, y_sems, (d - 1, 1), target),
+            send(down, down, y_sems, (d - 1, 2), target),
+        )
+
+    def by_window(owner, work):
+        pl.when(owner < n - 1)(lambda: work(chunk))
+        pl.when(owner == n - 1)(lambda: work(last))
+
+    def start_weights(d):
+        def work(size):
+            for copy in w_copies(d, size):
+                copy.start()
+
+        by_window(there(d), work)
+
+    def pass_weights(d):
+        def work(size):
+            for copy, forward in zip(w_copies(d, size), y_copies(d, size)):
+                copy.wait_recv()
+                forward.start()
+
+        by_window(me, work)
+
     for d in range(1, n):
 
-        @pl.when(me + d < n)
+        @pl.when(me + d >= n)
         def _(d=d):
-            for copy in kv_copies(d):
-                copy.start()
-
-    def w_copies(d):
-        j = there(d)
-        start = pl.multiple_of(jnp.minimum(j * chunk, ff - chunk), 128)
-        target = {"sp": j}
-        in_rows = pl.ds(pl.multiple_of(g * half, half), half)
-        in_cols = pl.ds(pl.multiple_of(g * dhalf, dhalf), dhalf)
-        return (
-            send(wg_ref.at[in_rows, pl.ds(start, chunk)], wg_all.at[d, in_rows], w_sems, (d - 1, 0), target),
-            send(wu_ref.at[in_rows, pl.ds(start, chunk)], wu_all.at[d, in_rows], w_sems, (d - 1, 1), target),
-            send(wd_ref.at[pl.ds(start, chunk), in_cols], wd_all.at[d, :, in_cols], w_sems, (d - 1, 2), target),
-        )
-
-    def y_copies(d):
-        target = {"grp": 1 - g}
-        in_rows = pl.ds(pl.multiple_of(g * half, half), half)
-        in_cols = pl.ds(pl.multiple_of(g * dhalf, dhalf), dhalf)
-        return (
-            send(wg_all.at[d, in_rows], wg_all.at[d, in_rows], y_sems, (d - 1, 0), target),
-            send(wu_all.at[d, in_rows], wu_all.at[d, in_rows], y_sems, (d - 1, 1), target),
-            send(wd_all.at[d, :, in_cols], wd_all.at[d, :, in_cols], y_sems, (d - 1, 2), target),
-        )
+            start_weights(d)
+
+    def own_weights(size):
+        mine = pl.ds(pl.multiple_of(me * chunk, 128), size)
+        wg_all[0, :, :size] = wg_ref[:, mine]
+        wu_all[0, :, :size] = wu_ref[:, mine]
+        wd_all[0, :size, :] = wd_ref[mine, :]
+        if size < chunk:
+            for d in range(n):
+                wg_all[d, :, size:] = jnp.zeros((depth, chunk - size), jnp.bfloat16)
+                wu_all[d, :, size:] = jnp.zeros((depth, chunk - size), jnp.bfloat16)
+                wd_all[d, size:, :] = jnp.zeros((chunk - size, dcols), jnp.bfloat16)
+
+    by_window(me, own_weights)
 
     for d in range(1, n):
-        for copy in w_copies(d):
-            copy.start()
-
-    mine = pl.multiple_of(jnp.minimum(me * chunk, ff - chunk), 128)
-    wg_all[0] = wg_ref[:, pl.ds(mine, chunk)]
-    wu_all[0] = wu_ref[:, pl.ds(mine, chunk)]
-    wd_all[0] = wd_ref[pl.ds(mine, chunk), :]
-
-    for d in range(1, n):
-
-        @pl.when(me + d < n)
-        def _(d=d):
-            for copy in kv_copies(d):
-                copy.wait_send()
+        if d == n - 1:
+            for e in range(1, n):
+
+                @pl.when(me + e < n)
+                def _(e=e):
+                    start_weights(e)
 
         @pl.when(me >= d)
         def _(d=d):
-            for copy in kv_copies(d):
+            arrived = kv_copies(d)
+            forwards = kv_copies(d + 1) if d + 1 < n else [None] * 3
+            for copy, forward in zip(arrived, forwards):
                 copy.wait_recv()
+                if forward is not None:
+                    pl.when(me + 1 < n)(forward.start)
 
         @pl.when(me < d)
         def _(d=d):
@@ -280,6 +318,7 @@
             joined = jnp.where(inside, summed / total, joined)
         att[:, cols] = joined.astype(jnp.bfloat16)
 
+    pass_weights(1)
     for k in range(width // 512):
         cols = slice(k * 512, (k + 1) * 512)
         proj[:, cols] = jnp.dot(
@@ -305,6 +344,8 @@
             proj[block(across(dx) * 2 + c), :].astype(jnp.float32) + pc_buf[dx].astype(jnp.float32)
         ).astype(jnp.bfloat16)
         px[dx].start()
+    if n > 2:
+        pass_weights(2)
     pc[0].wait_recv()
     acc = proj[block(t), :].astype(jnp.float32) + pc_buf[0].astype(jnp.float32)
     for dx in range(1, nx):
@@ -335,83 +376,92 @@
     spreads = [spread(d) for d in range(n)]
     for copy in spreads[0]:
         copy.start()
-    for d in range(1, n):
-        for copy, forward in zip(w_copies(d), y_copies(d)):
-            copy.wait_recv()
-            forward.start()
-    for dx in range(1, nx):
-        spreads[0][dx].wait_recv()
-        relay(0, dx).start()
+    for d in range(3, n):
+        pass_weights(d)
+
+    def relay_all(d):
+        for dx in range(1, nx):
+            spreads[d][dx].wait_recv()
+            relay(d, dx).start()
+
+    relay_all(0)
     for d in range(1, n):
         nz[d].wait_recv()
         for copy in spreads[d]:
             copy.start()
-    for d in range(1, n):
-        for dx in range(1, nx):
-            spreads[d][dx].wait_recv()
-            relay(d, dx).start()
-    for d in range(1, n):
-        for copy in y_copies(d):
-            copy.wait_recv()
-    for d in range(n):
+        if d > 1:
+            relay_all(d - 1)
+
+    def y_arrived(size):
+        for d in range(1, n):
+            for copy in y_copies(d, size):
+                copy.wait_recv()
+
+    by_window(me, y_arrived)
+
+    def c_copy(d, dx):
+        j = origin(d)
+        return send(
+            part.at[j, block(across(dx) * 2 + 1 - c)], c_buf.at[d, dx], c_sems, (d, dx), {"tp": mate}
+        )
+
+    def feed(d):
+        j = origin(d)
         spreads[d][0].wait_recv()
         for dx in range(1, nx):
             relay(d, dx).wait_recv()
-
-    skipped = me * chunk - mine
-    live = lax.broadcasted_iota(jnp.int32, (rows, chunk), 1) >= skipped
-    order = [d % n for d in range(1, n + 1)]
-
-    def c_copy(d, dx):
-        j = there(d)
-        return send(
-            part.at[j, block(across(dx) * 2 + 1 - c)], c_buf.at[d, dx], c_sems, (d, dx), {"tp": mate}
-        )
-
-    def feed(index, carry):
-        d = lax.rem(index + 1, n)
-        j = there(d)
         gate = jnp.zeros((rows, chunk), jnp.float32)
         up = jnp.zeros((rows, chunk), jnp.float32)
         for e in range(n):
             piece = normed[j, :, pl.ds(pl.multiple_of(origin(e) * depth, depth), depth)]
             gate += jnp.dot(piece, wg_all[e], preferred_element_type=jnp.float32)
             up += jnp.dot(piece, wu_all[e], preferred_element_type=jnp.float32)
-        value = gate / (1.0 + jnp.exp(-gate)) * up
-        hid[...] = jnp.where(live, value, 0.0).astype(jnp.bfloat16)
+        hid[...] = (gate / (1.0 + jnp.exp(-gate)) * up).astype(jnp.bfloat16)
         for e in range(n):
             part[j, :, pl.ds(pl.multiple_of(origin(e) * dcols, dcols), dcols)] = jnp.dot(
                 hid[...], wd_all[e], preferred_element_type=jnp.float32
             ).astype(jnp.bfloat16)
         for dx in range(nx):
             c_copy(d, dx).start()
-        return carry
-
-    lax.fori_loop(0, n, feed, 0)
 
     def x_copy(d, dx):
         return send(x_send.at[d, dx], x_buf.at[d, dx], x_sems, (d, dx), {"tp": across(dx) * 2 + c})
 
     def z_copy(d):
-        return send(z_send.at[d], z_buf.at[d], z_sems, (d,), {"sp": there(d)})
-
-    for d in order:
+        return send(z_send.at[d], z_buf.at[d], z_sems, (d,), {"sp": origin(d)})
+
+    def over_x(d):
         for dx in range(1, nx):
             c_copy(d, dx).wait_recv()
             x_send[d, dx] = (
-                part[there(d), block(across(dx) * 2 + c), :].astype(jnp.float32)
+                part[origin(d), block(across(dx) * 2 + c), :].astype(jnp.float32)
                 + c_buf[d, dx].astype(jnp.float32)
             ).astype(jnp.bfloat16)
             x_copy(d, dx).start()
-    for d in order:
+
+    def over_z(d):
         c_copy(d, 0).wait_recv()
-        acc = part[there(d), block(t), :].astype(jnp.float32) + c_buf[d, 0].astype(jnp.float32)
+        acc = part[origin(d), block(t), :].astype(jnp.float32) + c_buf[d, 0].astype(jnp.float32)
         for dx in range(1, nx):
             x_copy(d, dx).wait_recv()
             acc += x_buf[d, dx].astype(jnp.float32)
         if d != 0:
             z_send[d] = acc.astype(jnp.bfloat16)
             z_copy(d).start()
+        return acc
+
+    for d in range(n):
+        if d == n - 1:
+            relay_all(d)
+        feed(d)
+        if d > 0:
+            over_x(d - 1)
+        if d > 2:
+            over_z(d - 2)
+    over_x(n - 1)
+    for d in range(max(1, n - 2), n):
+        over_z(d)
+    acc = over_z(0)
     for d in range(1, n):
         z_copy(d).wait_recv()
         acc += z_buf[d].astype(jnp.float32)
@@ -434,10 +484,22 @@
     for d in range(1, n):
         nz[d].wait_send()
         z_copy(d).wait_send()
-        for copy in w_copies(d):
-            copy.wait_send()
-        for copy in y_copies(d):
-            copy.wait_send()
+
+        def w_sent(size, d=d):
+            for copy in w_copies(d, size):
+                copy.wait_send()
+
+        def y_sent(size, d=d):
+            for copy in y_copies(d, size):
+                copy.wait_send()
+
+        by_window(there(d), w_sent)
+        by_window(me, y_sent)
+
+        @pl.when((me >= d - 1) & (me + 1 < n))
+        def _(d=d):
+            for copy in kv_copies(d):
+                copy.wait_send()
 
 
 def fused_body(residual, queries, keys, values, log_gates, w_out, norm_gain, w_gate, w_up, w_down):

time: 164 us -> 147 us (0.90); the launches traced: 161 us -> 147 us
  Pallas kernels: 157 us -> 143 us
    pallas_call x1, Pallas kernels: 157 us -> 143 us  [fused_body(): pl.pallas_call(functools.partial(layer_kernel, n, tp, chunk), out_shape=j...]
where the time goes in v2:
time: 147 us
  Pallas kernels  143 us (97%)
  local copies, waits for them, and re-layouts  4.43 us (3%)
    pallas_call x1, Pallas kernels, fused_body(): pl.pallas_call(functools.partial(layer_kernel, n, tp, chunk), out_shape=j...  143 us
    unnamed x2, local copies, waits for them, and re-layouts  3.15 us

profile of v2, /device:TPU:17, one launch (start us, length us, event | category | flops | bytes accessed | tf_op | source)
XLA Modules:
  0.0 147.2 jit_solution(9363215559739556346)
XLA Ops:
  0.0 1.3 pad.4.gt_ref
  1.3 1.5 %copy.11.g_ref = f32[256,4]{1,0:T(8,128)} copy(f32[256,4]{0,1:T(4,128)} %param.14) | data formatting | bytes 8192 | tf_op args[4]
  2.8 142.7 %shard_map.100 = bf16[64,2048]{1,0:T(8,128)(2,1)} custom-call(bf16[256,256]{1,0:T(8,128)(2,1)} %q_ref.1, bf16[256,256]{1,0:T(8,128)(2,1)} %k_ref.1, bf16[256,256]{1,0:T(8,128)(2,1)} %v_ref.1, f32[256,4]{1,0:T(8,128)} %copy.11.g_ref, f32[8,256]{1,0:T(8,128)} %pad.4.gt_ref, bf16[256,2048]{1,0:T(8,128)(2,1)} %residual_ref.1, bf16[256,2048]{1,0:T(8,128)(2,1)} %w_out_ref.1, ...), custom_call_target="tpu_custom_call" | custom-call | tf_op jit(solution)/shard_map/pallas_call | solution.py:551
  145.5 1.7 %copy.13 = bf16[64,2048]{1,0:T(8,128)(2,1)} copy(bf16[64,2048]{1,0:T(8,128)(2,1)} %shard_map.100) | data formatting | bytes 524288

commit v3 on v2

--- a/solution.py
+++ b/solution.py
@@ -135,7 +135,7 @@
     out_ref,
     k_all, v_all, gt_all, att, proj, pc_buf, px_send, px_buf, mixed, normed,
     wg_all, wu_all, wd_all, hid, part, c_buf, x_send, x_buf, z_send, z_buf,
-    kv_sems, w_sems, y_sems, pc_sems, px_sems, nz_sems, nx_sems, nc_sems, c_sems, x_sems, z_sems,
+    kv_sems, w_sems, y_sems, pc_sems, px_sems, nz_sems, nx_sems, nc_sems, c_sems, x_sems, z_sems, o_sems,
 ):
     me = lax.axis_index("sp")
     t = lax.axis_index("tp")
@@ -240,11 +240,17 @@
         def _(d=d):
             start_weights(d)
 
+    def own_copies(size):
+        mine = pl.ds(pl.multiple_of(jnp.minimum(me * chunk, ff - size), 128), size)
+        return (
+            pltpu.make_async_copy(wg_ref.at[:, mine], wg_all.at[0, :, :size], o_sems.at[0]),
+            pltpu.make_async_copy(wu_ref.at[:, mine], wu_all.at[0, :, :size], o_sems.at[1]),
+            pltpu.make_async_copy(wd_ref.at[mine, :], wd_all.at[0, :size, :], o_sems.at[2]),
+        )
+
     def own_weights(size):
-        mine = pl.ds(pl.multiple_of(me * chunk, 128), size)
-        wg_all[0, :, :size] = wg_ref[:, mine]
-        wu_all[0, :, :size] = wu_ref[:, mine]
-        wd_all[0, :size, :] = wd_ref[mine, :]
+        for copy in own_copies(size):
+            copy.start()
         if size < chunk:
             for d in range(n):
                 wg_all[d, :, size:] = jnp.zeros((depth, chunk - size), jnp.bfloat16)
@@ -393,6 +399,8 @@
             relay_all(d - 1)
 
     def y_arrived(size):
+        for copy in own_copies(size):
+            copy.wait()
         for d in range(1, n):
             for copy in y_copies(d, size):
                 copy.wait_recv()
@@ -547,11 +555,13 @@
         (2, n, nx),
         (2, n, nx),
         (2, n),
+        (3,),
     ]
     return pl.pallas_call(
         functools.partial(layer_kernel, n, tp, chunk),
         out_shape=jax.ShapeDtypeStruct((sub, width), bf16),
-        in_specs=[pl.BlockSpec(memory_space=pltpu.VMEM)] * 11,
+        in_specs=[pl.BlockSpec(memory_space=pltpu.VMEM)] * 8
+        + [pl.BlockSpec(memory_space=pl.ANY)] * 3,
         out_specs=pl.BlockSpec(memory_space=pltpu.VMEM),
         scratch_shapes=[pltpu.VMEM(shape, dtype) for shape, dtype in shapes]
         + [pltpu.SemaphoreType.DMA(shape) for shape in sems],

time: 147 us -> 146 us (level)
  Pallas kernels: 143 us -> 141 us
where the time goes in v3:
time: 146 us
  Pallas kernels  141 us (97%)
  local copies, waits for them, and re-layouts  4.43 us (3%)
    pallas_call x1, Pallas kernels, fused_body(): pl.pallas_call(functools.partial(layer_kernel, n, tp, chunk), out_shape=j...  141 us
    unnamed x2, local copies, waits for them, and re-layouts  3.15 us

profile of v3, /device:TPU:17, one launch (start us, length us, event | category | flops | bytes accessed | tf_op | source)
XLA Modules:
  0.0 145.9 jit_solution(17174644291510654811)
XLA Ops:
  0.0 1.3 pad.4.gt_ref
  1.3 1.5 %copy.11.g_ref = f32[256,4]{1,0:T(8,128)} copy(f32[256,4]{0,1:T(4,128)} %param.14) | data formatting | bytes 8192 | tf_op args[4]
  2.8 141.4 %shard_map.100 = bf16[64,2048]{1,0:T(8,128)(2,1)} custom-call(bf16[256,256]{1,0:T(8,128)(2,1)} %q_ref.1, bf16[256,256]{1,0:T(8,128)(2,1)} %k_ref.1, bf16[256,256]{1,0:T(8,128)(2,1)} %v_ref.1, f32[256,4]{1,0:T(8,128)} %copy.11.g_ref, f32[8,256]{1,0:T(8,128)} %pad.4.gt_ref, bf16[256,2048]{1,0:T(8,128)(2,1)} %residual_ref.1, bf16[256,2048]{1,0:T(8,128)(2,1)} %w_out_ref.1, ...), custom_call_target="tpu_custom_call" | custom-call | tf_op jit(solution)/shard_map/pallas_call | solution.py:560
  144.2 1.7 %copy.13 = bf16[64,2048]{1,0:T(8,128)(2,1)} copy(bf16[64,2048]{1,0:T(8,128)(2,1)} %shard_map.100) | data formatting | bytes 524288
